TPU v7x, 32 devices: a whole 2x2x4 slice. The times are simulated.
32 devices in a mesh: ep: 8 (over z, core), tp: 4 (over y, x).
Axes of the slice: x: 2, y: 2, z: 4, core: 2. Of those that a mesh axis runs over, the one named last changes fastest.
Arguments:
- tokens: bfloat16 [128, 1024], P('ep'), may hold values from -6 to 6
- kv_cache: bfloat16 [128, 1024, 16, 128], P('ep', None, 'tp'), may hold values from -6 to 6
- lengths: int32 [128], P('ep'), may hold values from 1 to 1024, 65536 in all
- score_offset: float32 [16], P('tp'), may hold values from 3 to 9
- mixer_gain: float32 [1024], replicated, may hold values from 0.1 to 1.9
- query_weight: bfloat16 [1024, 1024], P(None, 'tp'), may hold values from -0.1875 to 0.1875
- key_weight: bfloat16 [1024, 1024], P(None, 'tp'), may hold values from -0.1875 to 0.1875
- value_weight: bfloat16 [1024, 1024], P(None, 'tp'), may hold values from -0.1875 to 0.1875
- out_weight: bfloat16 [1024, 1024], P('tp'), may hold values from -0.75 to 0.75
- channel_gain: float32 [1024], replicated, may hold values from 0.1 to 1.9
- routes: int32 [128, 2], P('ep'), may hold values from 0 to 7, all different within a row; in each aligned block of 16 rows (0 to 15, 16 to 31, ...) at most 8 rows name the same one
- route_weights: float32 [128, 2], P('ep'), may hold values from 0.25 to 1
- gate_weight: bfloat16 [8, 1024, 2048], P('ep', None, 'tp'), may hold values from -0.1875 to 0.1875
- up_weight: bfloat16 [8, 1024, 2048], P('ep', None, 'tp'), may hold values from -0.1875 to 0.1875
- down_weight: bfloat16 [8, 2048, 1024], P('ep', 'tp'), may hold values from -0.125 to 0.125
Outputs:
- mixed: bfloat16 [128, 1024], P('ep', 'tp')
- new_entries: bfloat16 [128, 16, 128], P('ep', 'tp')
Inputs may be any that keep to these rules, and one draw needn't show every extreme that they name: `routes`: each row names 2 different experts; within the rows of one index of ep (aligned blocks of 16 rows) no expert is named more than 8 times. `lengths`: some sequence fills all 1024 positions.
All inputs are finite; a program needn't handle non-finite values. No bound on the sum of `lengths` on one device may be relied on, other than what follows from the above.
Results may differ from a plain program's by a relative error of at most 0.017.
Values may be sent and summed in bfloat16 or wider, within the bound.
A program may use at most 128 MiB of HBM per device.

v0:
```python
import jax
import jax.numpy as jnp
from jax import lax
from jax.sharding import PartitionSpec as P

EPSILON = 1e-06


def rms_scale(values, scale_gain):
    return (
        values * lax.rsqrt(jnp.mean(values * values, axis=-1, keepdims=True) + EPSILON) * scale_gain
    )


def expert_apply(arrived_rows, gate_weight, up_weight, down_weight):
    gate_rows = jnp.dot(arrived_rows, gate_weight[0], preferred_element_type=jnp.float32)
    upward = jnp.dot(arrived_rows, up_weight[0], preferred_element_type=jnp.float32)
    active = (jax.nn.silu(gate_rows) * upward).astype(jnp.bfloat16)
    partial_rows = jnp.dot(active, down_weight[0], preferred_element_type=jnp.float32)
    return lax.psum_scatter(
        partial_rows.astype(jnp.bfloat16), "tp", scatter_dimension=1, tiled=True
    )


def per_device(
    tokens,
    kv_cache,
    lengths,
    score_offset,
    mixer_gain,
    query_weight,
    key_weight,
    value_weight,
    out_weight,
    channel_gain,
    routes,
    route_weights,
    gate_weight,
    up_weight,
    down_weight,
):
    seq_dev = tokens.shape[0]
    model_width = tokens.shape[1]
    experts = lax.axis_size("ep")
    top_count = routes.shape[1]
    capacity = max(2, 2 * seq_dev * top_count // experts)
    heads_dev = kv_cache.shape[2]
    head_dim = kv_cache.shape[3] // 2
    head_span = heads_dev * head_dim
    col_width = model_width // lax.axis_size("tp")
    col_start = lax.axis_index("tp") * col_width
    inputs = tokens.astype(jnp.float32)
    normed = rms_scale(inputs, mixer_gain).astype(jnp.bfloat16)
    query_rows = (
        jnp.dot(normed, query_weight, preferred_element_type=jnp.float32)
        .astype(jnp.bfloat16)
        .reshape(seq_dev, heads_dev, head_dim)
    )
    key_rows = (
        jnp.dot(normed, key_weight, preferred_element_type=jnp.float32)
        .astype(jnp.bfloat16)
        .reshape(seq_dev, heads_dev, head_dim)
    )
    value_rows = (
        jnp.dot(normed, value_weight, preferred_element_type=jnp.float32)
        .astype(jnp.bfloat16)
        .reshape(seq_dev, heads_dev, head_dim)
    )
    new_entries = jnp.concatenate([key_rows, value_rows], axis=2)
    cached_keys = kv_cache[..., :head_dim]
    cached_values = kv_cache[..., head_dim:]
    scores = (
        jnp.einsum("shd,sphd->shp", query_rows, cached_keys, preferred_element_type=jnp.float32)
        * head_dim ** (-0.5)
        - score_offset[None, :, None]
    )
    positions = jnp.arange(kv_cache.shape[1], dtype=jnp.int32)
    visible = (positions[None, :] < lengths[:, None])[:, None, :]
    log_keep = jnp.where(visible, jax.nn.log_sigmoid(-scores), 0.0)
    after_sum = lax.cumsum(log_keep, axis=2, reverse=True) - log_keep
    stick_weights = jnp.where(visible, jnp.exp(jax.nn.log_sigmoid(scores) + after_sum), 0.0).astype(
        jnp.bfloat16
    )
    attended = (
        jnp.einsum(
            "shp,sphd->shd", stick_weights, cached_values, preferred_element_type=jnp.float32
        )
        .astype(jnp.bfloat16)
        .reshape(seq_dev, head_span)
    )
    partial_out = jnp.dot(attended, out_weight, preferred_element_type=jnp.float32)
    mixed_heads = lax.psum(partial_out.astype(jnp.bfloat16), "tp").astype(jnp.float32)
    residual = inputs + mixed_heads
    hidden = rms_scale(residual, channel_gain).astype(jnp.bfloat16)
    residual_cols = lax.dynamic_slice_in_dim(residual, col_start, col_width, 1)
    flat_routes = routes.reshape(-1)
    pair_count = flat_routes.shape[0]
    pair_index = jnp.arange(pair_count, dtype=jnp.int32)
    earlier = (flat_routes[None, :] == flat_routes[:, None]) & (
        pair_index[None, :] < pair_index[:, None]
    )
    slot_rank = jnp.sum(earlier.astype(jnp.int32), axis=1)
    slot_index = flat_routes * capacity + slot_rank
    slot_table = (
        slot_index[:, None] == jnp.arange(experts * capacity, dtype=jnp.int32)[None, :]
    ).astype(jnp.bfloat16)
    token_table = (
        (pair_index // top_count)[:, None] == jnp.arange(seq_dev, dtype=jnp.int32)[None, :]
    ).astype(jnp.bfloat16)
    placing = lax.dot_general(
        slot_table, token_table, (((0,), (0,)), ((), ())), preferred_element_type=jnp.float32
    ).astype(jnp.bfloat16)
    outgoing = (
        jnp.dot(placing, hidden, preferred_element_type=jnp.float32)
        .astype(jnp.bfloat16)
        .reshape(experts, capacity, model_width)
    )
    arrived = lax.all_to_all(outgoing, "ep", split_axis=0, concat_axis=0, tiled=True)
    sources = arrived.shape[0]
    item_count = arrived.shape[1]
    served = expert_apply(
        arrived.reshape(sources * item_count, model_width), gate_weight, up_weight, down_weight
    )
    returned = lax.all_to_all(
        served.reshape(sources, item_count, col_width),
        "ep",
        split_axis=0,
        concat_axis=0,
        tiled=True,
    )
    picked = (
        jnp.take(returned.reshape(experts * capacity, col_width), slot_index, axis=0)
        .astype(jnp.float32)
        .reshape(seq_dev, top_count, col_width)
    )
    expert_mix = jnp.sum(route_weights[:, :, None] * picked, axis=1)
    mixed = (residual_cols + expert_mix).astype(jnp.bfloat16)
    return (mixed, new_entries)


def solution(mesh):
    placed = (
        P("ep", None),
        P("ep", None, "tp", None),
        P("ep"),
        P("tp"),
        P(),
        P(None, "tp"),
        P(None, "tp"),
        P(None, "tp"),
        P("tp", None),
        P(),
        P("ep", None),
        P("ep", None),
        P("ep", None, "tp"),
        P("ep", None, "tp"),
        P("ep", "tp", None),
    )
    return jax.shard_map(
        per_device,
        mesh=mesh,
        in_specs=placed,
        out_specs=(P("ep", "tp"), P("ep", "tp", None)),
        check_vma=False,
    )
```

profile of v0, /device:TPU:0, one launch (start us, length us, event | category | flops | bytes accessed | tf_op | source)
XLA Modules:
  0.0 204.8 jit_solution(8012853893740738243)
XLA Ops:
  7.2 0.0 copy-start
  7.2 0.0 copy-start.3
  7.2 0.0 copy-start.4
  7.2 0.0 copy-start.5
  7.2 0.0 copy-start.9
  7.2 23.2 %fusion.45 = (bf16[16,1024,4,64]{3,2,1,0:T(4,128)(2,1)}, bf16[16,1024,4,64]{3,2,1,0:T(4,128)(2,1)}) fusion(bf16[16,1024,4,128]{3,2,1,0:T(4,128)(2,1)} %param.16), kind=kLoop, calls=%fused_computation.78 | loop fusion | bytes 33554432 | tf_op jit(solution)/shard_map/slice | solution.py:70
  30.4 0.0 copy-done.3
  30.4 0.0 copy-start.7
  30.4 0.1 fusion.29
  30.6 0.0 copy-done.4
  30.6 0.0 copy-done.5
  30.6 0.2 convolution_convert_fusion.5
  30.8 0.1 reshape.164
  30.9 0.0 copy-done.9
  30.9 0.1 iota_compare_fusion
  31.0 10.2 %fusion.2 = f32[16,4,1,1024]{3,2,1,0:T(1,128)S(1)} fusion(bf16[16,4,64,1]{2,3,1,0:T(2,128)(2,1)S(1)} %reshape.164, bf16[16,1024,4,64]{3,2,1,0:T(4,128)(2,1)} %get-tuple-element.2), kind=kOutput, calls=%fused_computation.3 | convolution fusion | flops 8388608 | bytes 8658944 | tf_op jit(solution)/shard_map/shd,sphd->shp/dot_general | solution.py:73
  41.2 0.0 copy-done.7
  41.2 0.5 fusion.17
  41.7 0.1 reshape.141
  41.8 79.2 %reduce-window.6 = f32[16,4,8,128]{3,2,1,0:T(8,128)S(1)} reduce-window(f32[16,4,8,128]{3,2,1,0:T(8,128)S(1)} %reshape.141, f32[]{:T(128)} %constant.46.clone.1), window={size=1x1x1x128 pad=0_0x0_0x0_0x0_127}, to_apply=%region_1.2 | reduce-window | flops 8323072 | bytes 524292 | tf_op jit(solution)/shard_map/reduce-window
  121.0 0.3 copy.30
  121.3 0.1 copy.31
  121.4 0.1 broadcast_add_fusion
  121.6 0.1 reduce_window_sum.15
  121.7 0.9 fusion.28
  122.5 0.0 copy-start.1
  122.5 0.0 copy-start.2
  122.5 0.0 copy-start.8
  122.6 8.3 %fusion = f32[16,4,1,64]{3,2,1,0:T(1,128)S(1)} fusion(bf16[16,1024,4,64]{3,2,1,0:T(4,128)(2,1)} %get-tuple-element.3, bf16[16,4,1024,1]{2,1,0,3:T(4,128)(2,1)S(1)} %fusion.28), kind=kOutput, calls=%fused_computation.1 | convolution fusion | flops 8388608 | bytes 8536064 | tf_op jit(solution)/shard_map/shp,sphd->shd/dot_general | solution.py:85
  130.8 0.1 reshape.143
  130.9 1.2 convolution_convert_fusion.2
  132.2 17.8 %psum.7 = bf16[16,1024]{1,0:T(8,128)(2,1)S(1)} all-reduce(bf16[16,1024]{1,0:T(8,128)(2,1)S(1)} %convolution_convert_fusion.2), channel_id=1, replica_groups=mesh['ep'=8,'tp'=4] {'tp'}, use_global_device_ids=true, to_apply=%region_3.4 | all-reduce | flops 16384 | bytes 65536 | tf_op jit(solution)/shard_map/psum | solution.py:92
  149.9 0.1 convert_add_fusion
  150.1 0.0 copy-done.6
  150.1 0.1 copy.33
  150.2 0.1 reshape.144
  150.3 0.2 convert_reduce_fusion
  150.4 0.0 copy-done.10
  150.5 1.1 fusion.4
  151.6 4.9 %all-to-all-start = ((bf16[8,8,1024]{2,1,0:T(8,128)(2,1)}), bf16[8,8,1024]{2,1,0:T(8,128)(2,1)S(1)}, u32[]{:S(2)}, u32[]{:S(2)}) async-start(bf16[8,8,1024]{2,1,0:T(8,128)(2,1)} %fusion.4), calls=%async_computation | async-start | bytes 262144 | tf_op jit(solution)/shard_map/all_to_all | solution.py:118
  156.4 0.0 reduce-scatter.2.cloned.1.call-start
  156.5 1.3 convolution_convert_fusion.3
  157.7 1.3 convolution_convert_fusion.4
  159.0 0.1 reduce_sum.42
  159.1 0.1 copy.34
  159.2 0.1 reshape.150
  159.3 0.1 reshape.149
  159.4 3.8 %all-to-all-done = bf16[8,8,1024]{2,1,0:T(8,128)(2,1)S(1)} async-done(((bf16[8,8,1024]{2,1,0:T(8,128)(2,1)}), bf16[8,8,1024]{2,1,0:T(8,128)(2,1)S(1)}, u32[]{:S(2)}, u32[]{:S(2)}) %all-to-all-start) | async-done | bytes 131104 | tf_op jit(solution)/shard_map/all_to_all | solution.py:118
  163.2 0.0 copy-done.1
  163.2 0.3 fusion.9
  163.5 1.2 convolution_convert_fusion
  164.7 0.0 reduce-scatter.2.cloned.1.call-update
  164.7 0.7 pad_maximum_fusion
  165.4 0.1 copy.36
  165.5 0.1 mul.108
  165.6 0.1 copy.35
  165.7 0.0 copy-done.8
  165.7 0.1 copy.32
  165.8 20.5 %reduce-scatter.2.cloned.1.call-done = bf16[64,256]{1,0:T(8,128)(2,1)} async-done(((bf16[64,1024]{1,0:T(8,128)(2,1)}), bf16[64,256]{1,0:T(8,128)(2,1)}) %reduce-scatter.2.cloned.1.call-update) | async-done | bytes 32784 | tf_op jit(solution)/shard_map/reduce_scatter | solution.py:20
  186.3 4.6 %all-to-all-start.1 = ((bf16[8,8,256]{2,1,0:T(8,128)(2,1)}), bf16[8,8,256]{2,1,0:T(8,128)(2,1)S(1)}, u32[]{:S(2)}, u32[]{:S(2)}) async-start(bf16[8,8,256]{2,1,0:T(8,128)(2,1)} %bitcast.56), calls=%async_computation.2 | async-start | bytes 65536 | tf_op jit(solution)/shard_map/all_to_all | solution.py:124
  190.9 5.7 %all-to-all-done.1 = bf16[8,8,256]{2,1,0:T(8,128)(2,1)S(1)} async-done(((bf16[8,8,256]{2,1,0:T(8,128)(2,1)}), bf16[8,8,256]{2,1,0:T(8,128)(2,1)S(1)}, u32[]{:S(2)}, u32[]{:S(2)}) %all-to-all-start.1) | async-done | bytes 32800 | tf_op jit(solution)/shard_map/all_to_all | solution.py:124
  196.6 0.6 gather_fusion
  197.3 0.1 multiply_reduce_fusion.1
  197.4 0.6 add_convert_fusion
  (15 shorter events, 0.1 us)
Async XLA Ops:
  7.2 156.3 %copy-start = (bf16[1,512,1024]{2,1,0:T(8,128)(2,1)S(1)}, bf16[1,512,1024]{2,1,0:T(8,128)(2,1)}, u32[]{:S(2)}) copy-start(bf16[1,512,1024]{2,1,0:T(8,128)(2,1)} %param.29) | copy-start | bytes 3145732
  7.2 23.2 %copy-start.3 = (bf16[16,1024]{1,0:T(8,128)(2,1)S(1)}, bf16[16,1024]{1,0:T(8,128)(2,1)}, u32[]{:S(2)}) copy-start(bf16[16,1024]{1,0:T(8,128)(2,1)} %param.15) | copy-start | bytes 98308
  7.2 23.4 %copy-start.4 = (bf16[1024,256]{1,0:T(8,128)(2,1)S(1)}, bf16[1024,256]{1,0:T(8,128)(2,1)}, u32[]{:S(2)}) copy-start(bf16[1024,256]{1,0:T(8,128)(2,1)} %param.20) | copy-start | bytes 1572868
  7.2 23.4 %copy-start.5 = (f32[1024]{0:T(1024)S(1)}, f32[1024]{0:T(1024)}, u32[]{:S(2)}) copy-start(f32[1024]{0:T(1024)} %param.19) | copy-start | bytes 12292
  7.2 23.7 %copy-start.9 = (s32[16]{0:T(128)S(1)}, s32[16]{0:T(128)}, u32[]{:S(2)}) copy-start(s32[16]{0:T(128)} %param.17) | copy-start | bytes 196
  30.4 10.8 %copy-start.7 = (f32[4]{0:T(128)S(1)}, f32[4]{0:T(128)}, u32[]{:S(2)}) copy-start(f32[4]{0:T(128)} %param.18) | copy-start | bytes 52
  121.4 28.7 %copy-start.6 = (s32[16,2]{0,1:T(2,128)S(1)}, s32[16,2]{0,1:T(2,128)}, u32[]{:S(2)}) copy-start(s32[16,2]{0,1:T(2,128)} %param.25) | copy-start | bytes 388
  121.4 29.0 %copy-start.10 = (f32[1024]{0:T(1024)S(1)}, f32[1024]{0:T(1024)}, u32[]{:S(2)}) copy-start(f32[1024]{0:T(1024)} %param.24) | copy-start | bytes 12292
  122.5 40.7 %copy-start.1 = (bf16[1,1024,512]{2,1,0:T(8,128)(2,1)S(1)}, bf16[1,1024,512]{2,1,0:T(8,128)(2,1)}, u32[]{:S(2)}) copy-start(bf16[1,1024,512]{2,1,0:T(8,128)(2,1)} %param.27) | copy-start | bytes 3145732
  122.5 41.0 %copy-start.2 = (bf16[1,1024,512]{2,1,0:T(8,128)(2,1)S(1)}, bf16[1,1024,512]{2,1,0:T(8,128)(2,1)}, u32[]{:S(2)}) copy-start(bf16[1,1024,512]{2,1,0:T(8,128)(2,1)} %param.28) | copy-start | bytes 3145732
  122.5 43.2 %copy-start.8 = (f32[16,2]{0,1:T(2,128)S(1)}, f32[16,2]{0,1:T(2,128)}, u32[]{:S(2)}) copy-start(f32[16,2]{0,1:T(2,128)} %param.26) | copy-start | bytes 388
  151.6 11.6 %all-to-all-start = ((bf16[8,8,1024]{2,1,0:T(8,128)(2,1)}), bf16[8,8,1024]{2,1,0:T(8,128)(2,1)S(1)}, u32[]{:S(2)}, u32[]{:S(2)}) async-start(bf16[8,8,1024]{2,1,0:T(8,128)(2,1)} %fusion.4), calls=%async_computation | async-start | bytes 262144 | tf_op jit(solution)/shard_map/all_to_all | solution.py:118
  156.4 29.8 %reduce-scatter.2.cloned.1.call-start = ((), (), s32[]{:S(2)}) async-start(), calls=%async_computation.3 | async-start | bytes 163840 | tf_op jit(solution)/shard_map/reduce_scatter | solution.py:20
  186.3 10.3 %all-to-all-start.1 = ((bf16[8,8,256]{2,1,0:T(8,128)(2,1)}), bf16[8,8,256]{2,1,0:T(8,128)(2,1)S(1)}, u32[]{:S(2)}, u32[]{:S(2)}) async-start(bf16[8,8,256]{2,1,0:T(8,128)(2,1)} %bitcast.56), calls=%async_computation.2 | async-start | bytes 65536 | tf_op jit(solution)/shard_map/all_to_all | solution.py:124
Sparse Core Ops, SparseCore 0:
  164.8 21.3 reduce-scatter.1
where the time goes:
time: 205 us
  other arithmetic  82.7 us (40%)
  waiting for transfers between devices  30 us (15%)
  local copies, waits for them, and re-layouts  25.5 us (12%)
  matrix products  25 us (12%)
  blocking collectives  17.8 us (9%)
  between operations  14.3 us (7%)
  starting transfers between devices  9.51 us (5%)
    another operation x2, other arithmetic  79.3 us
    slice x1, local copies, waits for them, and re-layouts, per_device(): cached_keys = kv_cache[..., :head_dim]  23.2 us
    reduce_scatter x1, waiting for transfers between devices, expert_apply(): lax.psum_scatter(partial_rows.astype(jnp.bfloat16), 'tp', scatter_dimensi...  20.5 us
    psum x1, blocking collectives, per_device(): lax.psum(partial_out.astype(jnp.bfloat16), 'tp').astype(jnp.float32)  17.8 us
    dot_general x1, matrix products, per_device(): jnp.einsum('shd,sphd->shp', query_rows, cached_keys, preferred_element_ty...  10.2 us
    dot_general x1, matrix products, per_device(): jnp.einsum('shp,sphd->shd', stick_weights, cached_values, preferred_eleme...  8.27 us
    all_to_all x1, waiting for transfers between devices, per_device(): lax.all_to_all(served.reshape(sources, item_count, col_width), 'ep', spli...  5.73 us
    all_to_all x1, starting transfers between devices, per_device(): lax.all_to_all(outgoing, 'ep', split_axis=0, concat_axis=0, tiled=True)  4.88 us
  transfers between devices with their start and end apart: 3, of which 3 were waited for; matrix products, arithmetic and copies ran while one was open for 2% of the time, Pallas kernels for 0%

commit v1 on v0

--- a/solution.py
+++ b/solution.py
@@ -1,6 +1,8 @@
 import jax
 import jax.numpy as jnp
 from jax import lax
+from jax.experimental import pallas as pl
+from jax.experimental.pallas import tpu as pltpu
 from jax.sharding import PartitionSpec as P
 
 EPSILON = 1e-06
@@ -9,6 +11,214 @@
 def rms_scale(values, scale_gain):
     return (
         values * lax.rsqrt(jnp.mean(values * values, axis=-1, keepdims=True) + EPSILON) * scale_gain
+    )
+
+
+def attend_kernel(
+    lengths_ref,
+    tokens_ref,
+    gain_ref,
+    offset_ref,
+    length_rows_ref,
+    query_hbm,
+    key_hbm,
+    value_hbm,
+    out_hbm,
+    cache_hbm,
+    partial_ref,
+    entries_ref,
+    cache_buf,
+    weight_buf,
+    out_buf,
+    query_scr,
+    score_scr,
+    sum_scr,
+    entry_scr,
+    weight_sem,
+    cache_sem,
+):
+    seqs, rows_all, lanes = cache_buf.shape
+    heads = entries_ref.shape[1]
+    head_dim = lanes // 2
+    parts = cache_sem.shape[1]
+    part_rows = rows_all // parts
+    part_span = part_rows // heads
+    blocks = rows_all // lanes
+    block_span = lanes // heads
+
+    def weight_copy(source, target, index):
+        return pltpu.make_async_copy(source, target, weight_sem.at[index])
+
+    copies = [
+        weight_copy(query_hbm, weight_buf.at[0], 0),
+        weight_copy(key_hbm, weight_buf.at[1], 1),
+        weight_copy(value_hbm, weight_buf.at[2], 2),
+        weight_copy(out_hbm, out_buf, 3),
+    ]
+    copies[0].start()
+
+    def cache_copy(seq, part):
+        span = pl.ds(part * part_rows, part_rows)
+        return pltpu.make_async_copy(
+            cache_hbm.at[seq, span], cache_buf.at[seq, span], cache_sem.at[seq, part]
+        )
+
+    def start_seq(seq, carry):
+        for part in range(parts):
+
+            @pl.when(lengths_ref[seq] > part * part_span)
+            def _():
+                cache_copy(seq, part).start()
+
+        return carry
+
+    lax.fori_loop(0, 2, start_seq, 0)
+    copies[1].start()
+    copies[2].start()
+    lax.fori_loop(2, seqs, start_seq, 0)
+    copies[3].start()
+
+    inputs = tokens_ref[...].astype(jnp.float32)
+    normed = rms_scale(inputs, gain_ref[...]).astype(jnp.bfloat16)
+    query_scr[...] = jnp.zeros_like(query_scr)
+    sum_scr[...] = jnp.zeros_like(sum_scr)
+    copies[0].wait()
+    query = jnp.dot(normed, weight_buf[0], preferred_element_type=jnp.float32)
+    for head in range(heads):
+        query_scr[:, head, :head_dim] = query[:, head * head_dim : (head + 1) * head_dim]
+
+    group = query_scr.shape[1]
+    row_id = lax.broadcasted_iota(jnp.int32, (group, part_rows), 0)
+    lane_id = lax.broadcasted_iota(jnp.int32, (group, part_rows), 1)
+    own_head = row_id == lane_id % heads
+
+    def score_seq(seq, carry):
+        query_rows = query_scr[seq].astype(jnp.bfloat16)
+        for part in range(parts):
+
+            @pl.when(lengths_ref[seq] > part * part_span)
+            def _():
+                cache_copy(seq, part).wait()
+                rows = cache_buf[seq, part * part_rows : (part + 1) * part_rows, :]
+                every = lax.dot_general(
+                    query_rows, rows, (((1,), (1,)), ((), ())), preferred_element_type=jnp.float32
+                )
+                score_scr[pl.ds(seq, 1), part * part_rows : (part + 1) * part_rows] = jnp.sum(
+                    jnp.where(own_head, every, 0.0), axis=0, keepdims=True
+                )
+
+        return carry
+
+    lax.fori_loop(0, seqs, score_seq, 0)
+
+    length_rows = length_rows_ref[...]
+    offsets = offset_ref[...]
+    lane = lax.broadcasted_iota(jnp.int32, (seqs, lanes), 1) // heads
+    scores, keeps = [], []
+    for block in range(blocks):
+        visible = lane + block * block_span < length_rows
+        score = score_scr[:, block * lanes : (block + 1) * lanes] * head_dim ** (-0.5) - offsets
+        score = jnp.where(visible, score, 0.0)
+        keep = -(jnp.maximum(score, 0.0) + jnp.log(1.0 + jnp.exp(-jnp.abs(score))))
+        keep = jnp.where(visible, keep, 0.0)
+        score_scr[:, block * lanes : (block + 1) * lanes] = score + keep
+        keeps.append(keep)
+    keep_all = jnp.concatenate(keeps, axis=0)
+    keep_high = keep_all.astype(jnp.bfloat16)
+    keep_low = (keep_all - keep_high.astype(jnp.float32)).astype(jnp.bfloat16)
+    from_id = lax.broadcasted_iota(jnp.int32, (2 * lanes, 2 * lanes), 0) % lanes
+    to_id = lax.broadcasted_iota(jnp.int32, (2 * lanes, 2 * lanes), 1)
+    same = from_id % heads == to_id % heads
+    later = (to_id >= lanes) | (from_id // heads > (to_id % lanes) // heads)
+    summing = jnp.where(same & later, 1.0, 0.0).astype(jnp.bfloat16)
+    summed = jnp.dot(
+        jnp.concatenate([keep_high, keep_low], axis=1), summing, preferred_element_type=jnp.float32
+    )
+    carry = jnp.zeros((seqs, lanes), jnp.float32)
+    for block in reversed(range(blocks)):
+        visible = lane + block * block_span < length_rows
+        piece = summed[block * seqs : (block + 1) * seqs]
+        exponent = score_scr[:, block * lanes : (block + 1) * lanes] + piece[:, :lanes] + carry
+        score_scr[:, block * lanes : (block + 1) * lanes] = jnp.where(
+            visible, jnp.exp(exponent), 0.0
+        )
+        carry = carry + piece[:, lanes:]
+
+    def value_seq(seq, carry):
+        for part in range(parts):
+
+            @pl.when(lengths_ref[seq] > part * part_span)
+            def _():
+                rows = cache_buf[seq, part * part_rows : (part + 1) * part_rows, :]
+                sticks = score_scr[pl.ds(seq, 1), part * part_rows : (part + 1) * part_rows]
+                sticks = jnp.where(
+                    own_head, jnp.broadcast_to(sticks, own_head.shape), 0.0
+                ).astype(jnp.bfloat16)
+                sum_scr[seq] += jnp.dot(sticks, rows, preferred_element_type=jnp.float32)
+
+        return carry
+
+    lax.fori_loop(0, seqs, value_seq, 0)
+
+    copies[1].wait()
+    copies[2].wait()
+    key = jnp.dot(normed, weight_buf[1], preferred_element_type=jnp.float32)
+    value = jnp.dot(normed, weight_buf[2], preferred_element_type=jnp.float32)
+    for head in range(heads):
+        span = slice(head * head_dim, (head + 1) * head_dim)
+        entry_scr[:, head, :] = jnp.concatenate([key[:, span], value[:, span]], axis=1)
+    entries_ref[...] = entry_scr[...].astype(entries_ref.dtype)
+
+    attended = jnp.concatenate(
+        [sum_scr[:, head, head_dim:] for head in range(heads)], axis=1
+    ).astype(jnp.bfloat16)
+    copies[3].wait()
+    partial_ref[...] = jnp.dot(
+        attended, out_buf[...], preferred_element_type=jnp.float32
+    ).astype(partial_ref.dtype)
+
+
+def attend(
+    tokens, kv_cache, lengths, score_offset, mixer_gain, query_weight, key_weight, value_weight, out_weight
+):
+    seqs, span, heads, lanes = kv_cache.shape
+    width = tokens.shape[1]
+    columns = query_weight.shape[1]
+    parts = 4 if span % 4 == 0 and (span // 4 * heads) % lanes == 0 else 1
+    vmem = pl.BlockSpec(memory_space=pltpu.VMEM)
+    hbm = pl.BlockSpec(memory_space=pl.ANY)
+    return pl.pallas_call(
+        attend_kernel,
+        name="attend",
+        out_shape=(
+            jax.ShapeDtypeStruct((seqs, width), jnp.bfloat16),
+            jax.ShapeDtypeStruct((seqs, heads, lanes), jnp.bfloat16),
+        ),
+        in_specs=[pl.BlockSpec(memory_space=pltpu.SMEM)] + [vmem] * 4 + [hbm] * 5,
+        out_specs=(vmem, vmem),
+        scratch_shapes=[
+            pltpu.VMEM((seqs, span * heads, lanes), jnp.bfloat16),
+            pltpu.VMEM((3, width, columns), jnp.bfloat16),
+            pltpu.VMEM(out_weight.shape, jnp.bfloat16),
+            pltpu.VMEM((seqs, 8, lanes), jnp.float32),
+            pltpu.VMEM((seqs, span * heads), jnp.float32),
+            pltpu.VMEM((seqs, 8, lanes), jnp.float32),
+            pltpu.VMEM((seqs, heads, lanes), jnp.float32),
+            pltpu.SemaphoreType.DMA((4,)),
+            pltpu.SemaphoreType.DMA((seqs, parts)),
+        ],
+        compiler_params=pltpu.CompilerParams(vmem_limit_bytes=48 * 1024 * 1024),
+    )(
+        lengths,
+        tokens,
+        mixer_gain[None, :],
+        jnp.tile(score_offset, lanes // heads)[None, :],
+        jnp.broadcast_to(lengths[:, None], (seqs, lanes)),
+        query_weight,
+        key_weight,
+        value_weight,
+        out_weight,
+        kv_cache.reshape(seqs, span * heads, lanes),
     )
 
 
@@ -44,52 +254,13 @@
     experts = lax.axis_size("ep")
     top_count = routes.shape[1]
     capacity = max(2, 2 * seq_dev * top_count // experts)
-    heads_dev = kv_cache.shape[2]
-    head_dim = kv_cache.shape[3] // 2
-    head_span = heads_dev * head_dim
     col_width = model_width // lax.axis_size("tp")
     col_start = lax.axis_index("tp") * col_width
     inputs = tokens.astype(jnp.float32)
-    normed = rms_scale(inputs, mixer_gain).astype(jnp.bfloat16)
-    query_rows = (
-        jnp.dot(normed, query_weight, preferred_element_type=jnp.float32)
-        .astype(jnp.bfloat16)
-        .reshape(seq_dev, heads_dev, head_dim)
-    )
-    key_rows = (
-        jnp.dot(normed, key_weight, preferred_element_type=jnp.float32)
-        .astype(jnp.bfloat16)
-        .reshape(seq_dev, heads_dev, head_dim)
-    )
-    value_rows = (
-        jnp.dot(normed, value_weight, preferred_element_type=jnp.float32)
-        .astype(jnp.bfloat16)
-        .reshape(seq_dev, heads_dev, head_dim)
-    )
-    new_entries = jnp.concatenate([key_rows, value_rows], axis=2)
-    cached_keys = kv_cache[..., :head_dim]
-    cached_values = kv_cache[..., head_dim:]
-    scores = (
-        jnp.einsum("shd,sphd->shp", query_rows, cached_keys, preferred_element_type=jnp.float32)
-        * head_dim ** (-0.5)
-        - score_offset[None, :, None]
-    )
-    positions = jnp.arange(kv_cache.shape[1], dtype=jnp.int32)
-    visible = (positions[None, :] < lengths[:, None])[:, None, :]
-    log_keep = jnp.where(visible, jax.nn.log_sigmoid(-scores), 0.0)
-    after_sum = lax.cumsum(log_keep, axis=2, reverse=True) - log_keep
-    stick_weights = jnp.where(visible, jnp.exp(jax.nn.log_sigmoid(scores) + after_sum), 0.0).astype(
-        jnp.bfloat16
-    )
-    attended = (
-        jnp.einsum(
-            "shp,sphd->shd", stick_weights, cached_values, preferred_element_type=jnp.float32
-        )
-        .astype(jnp.bfloat16)
-        .reshape(seq_dev, head_span)
-    )
-    partial_out = jnp.dot(attended, out_weight, preferred_element_type=jnp.float32)
-    mixed_heads = lax.psum(partial_out.astype(jnp.bfloat16), "tp").astype(jnp.float32)
+    partial_out, new_entries = attend(
+        tokens, kv_cache, lengths, score_offset, mixer_gain, query_weight, key_weight, value_weight, out_weight
+    )
+    mixed_heads = lax.psum(partial_out, "tp").astype(jnp.float32)
     residual = inputs + mixed_heads
     hidden = rms_scale(residual, channel_gain).astype(jnp.bfloat16)
     residual_cols = lax.dynamic_slice_in_dim(residual, col_start, col_width, 1)

time: 205 us -> 107 us (0.52)
  other arithmetic: 82.7 us -> 1.08 us
  matrix products: 25 us -> 2.6 us
  Pallas kernels: 0 us -> 16.5 us
  local copies, waits for them, and re-layouts: 25.5 us -> 9.87 us
  waiting for transfers between devices: 30 us -> 33.5 us
    another operation x3 -> x0, other arithmetic: 79.4 us -> none
    slice x2 -> x0, local copies, waits for them, and re-layouts: 23.5 us -> none  [the longest x1 23.2 us: per_device(): cached_keys = kv_cache[..., :head_dim]]
    dot_general x6 -> x0, matrix products: 22.4 us -> none  [the longest x1 10.2 us: per_device(): jnp.einsum('shd,sphd->shp', query_rows, cached_keys, preferred_element_ty...]
    pallas_call x0 -> x1, Pallas kernels: none -> 16.5 us  [attend(): pl.pallas_call(attend_kernel, name='attend', out_shape=(jax.ShapeDtypeStr...]
    unnamed x24 -> x30, local copies, waits for them, and re-layouts: 0.23 us -> 7.22 us
    all_to_all x1, waiting for transfers between devices: 3.8 us -> 6.51 us  [per_device(): lax.all_to_all(outgoing, 'ep', split_axis=0, concat_axis=0, tiled=True)]
  transfers between devices with their start and end apart: 3 -> 3, of which waited for: 3 -> 3; matrix products, arithmetic and copies ran while one was open for 2% -> 1% of each run, Pallas kernels for 0% -> 0%
where the time goes in v1:
time: 107 us; the launch traced here: 106 us
  waiting for transfers between devices  33.5 us (31%)
  blocking collectives  17.8 us (17%)
  Pallas kernels  16.5 us (15%)
  between operations  14.2 us (13%)
  starting transfers between devices  10.8 us (10%)
  local copies, waits for them, and re-layouts  9.87 us (9%)
  matrix products  2.6 us (2%)
  other arithmetic  1.08 us (1%)
    reduce_scatter x1, waiting for transfers between devices, expert_apply(): lax.psum_scatter(partial_rows.astype(jnp.bfloat16), 'tp', scatter_dimensi...  21.3 us
    psum x1, blocking collectives, per_device(): mixed_heads = lax.psum(partial_out, 'tp').astype(jnp.float32)  17.8 us
    pallas_call x1, Pallas kernels, attend(): pl.pallas_call(attend_kernel, name='attend', out_shape=(jax.ShapeDtypeStr...  16.5 us
    unnamed x30, local copies, waits for them, and re-layouts  7.22 us
    all_to_all x1, waiting for transfers between devices, per_device(): lax.all_to_all(outgoing, 'ep', split_axis=0, concat_axis=0, tiled=True)  6.51 us
    all_to_all x1, starting transfers between devices, per_device(): lax.all_to_all(outgoing, 'ep', split_axis=0, concat_axis=0, tiled=True)  6.2 us
    all_to_all x1, waiting for transfers between devices, per_device(): lax.all_to_all(served.reshape(sources, item_count, col_width), 'ep', spli...  5.73 us
    all_to_all x1, starting transfers between devices, per_device(): lax.all_to_all(served.reshape(sources, item_count, col_width), 'ep', spli...  4.59 us
  transfers between devices with their start and end apart: 3, of which 3 were waited for; matrix products, arithmetic and copies ran while one was open for 1% of the time, Pallas kernels for 0%

profile of v1, /device:TPU:0, one launch (start us, length us, event | category | flops | bytes accessed | tf_op | source)
XLA Modules:
  0.0 106.4 jit_solution(6702310970512895902)
XLA Ops:
  7.2 0.0 copy-start
  7.2 0.0 copy-start.11
  7.2 0.0 copy-start.6
  7.2 0.0 copy-start.13
  7.2 0.0 copy-start.12
  7.2 0.8 copy.27
  8.1 0.1 reshape.97
  8.1 0.2 convert_reduce_fusion
  8.3 0.7 tile.2
  9.0 0.1 broadcast_in_dim_tile.3.offset_ref
  9.1 0.7 broadcast_in_dim.12.length_rows_ref
  9.8 0.0 copy-start.1
  9.8 1.0 copy-done.1
  10.9 0.0 copy-start.2
  10.9 1.0 copy-done.2
  11.9 0.0 copy-start.3
  11.9 1.0 copy-done.3
  13.0 0.0 copy-start.4
  13.0 1.0 copy-done.4
  14.0 0.0 copy-start.5
  14.0 0.8 copy-done.5
  14.8 0.0 copy-start.7
  14.8 0.7 copy-done.7
  15.5 0.0 copy-start.8
  15.5 0.7 copy-done.8
  16.1 0.0 copy-start.9
  16.1 0.0 copy-start.10
  16.1 16.5 %attend.1 = (bf16[16,1024]{1,0:T(8,128)(2,1)S(1)}, bf16[16,4,128]{2,1,0:T(4,128)(2,1)}) custom-call(s32[16]{0:T(128)S(1)} %copy-done.8, bf16[16,1024]{1,0:T(8,128)(2,1)S(1)} %copy-done.5, f32[1,1024]{1,0:T(1,128)S(1)} %bitcast.28, f32[1,128]{1,0:T(1,128)S(1)} %broadcast_in_dim_tile.3.offset_ref, s32[16,128]{1,0:T(8,128)S(1)} %broadcast_in_dim.12.length_rows_ref, ...), custom_call_target="tpu_custom_call" | custom-call | tf_op jit(solution)/shard_map/attend/pallas_call | solution.py:190
  32.6 17.8 %psum.7 = bf16[16,1024]{1,0:T(8,128)(2,1)S(1)} all-reduce(bf16[16,1024]{1,0:T(8,128)(2,1)S(1)} %get-tuple-element.4), channel_id=1, replica_groups=mesh['ep'=8,'tp'=4] {'tp'}, use_global_device_ids=true, to_apply=%region_0.0 | all-reduce | flops 16384 | bytes 65536 | tf_op jit(solution)/shard_map/psum | solution.py:263
  50.4 0.0 copy-done.6
  50.5 0.1 convert_add_fusion
  50.6 0.0 copy-done.13
  50.6 1.1 %fusion = bf16[8,8,1024]{2,1,0:T(8,128)(2,1)} fusion(f32[1024]{0:T(1024)S(1)} %copy-done.13, f32[16]{0:T(128)S(1)} %add_rsqrt_fusion, s32[32]{0:T(128)S(1)} %get-tuple-element.8, s32[32]{0:T(128)S(1)} %get-tuple-element.9, bf16[16,1024]{1,0:T(8,128)(2,1)S(1)} %psum.7, bf16[16,1024]{1,0:T(8,128)(2,1)S(1)} %copy-done.6), kind=kOutput, calls=%fused_computation.4 | convolution fusion | flops 2330112 | bytes 201024 | tf_op jit(solution)/shard_map/dot_general | solution.py:285
  51.7 6.2 %all-to-all-start = ((bf16[8,8,1024]{2,1,0:T(8,128)(2,1)}), bf16[8,8,1024]{2,1,0:T(8,128)(2,1)S(1)}, u32[]{:S(2)}, u32[]{:S(2)}) async-start(bf16[8,8,1024]{2,1,0:T(8,128)(2,1)} %fusion), calls=%async_computation | async-start | bytes 262144 | tf_op jit(solution)/shard_map/all_to_all | solution.py:289
  57.9 0.0 reduce-scatter.2.cloned.1.call-start
  58.0 0.1 reduce_sum.32
  58.0 0.1 copy.28
  58.1 0.0 copy-done.11
  58.1 6.5 %all-to-all-done = bf16[8,8,1024]{2,1,0:T(8,128)(2,1)S(1)} async-done(((bf16[8,8,1024]{2,1,0:T(8,128)(2,1)}), bf16[8,8,1024]{2,1,0:T(8,128)(2,1)S(1)}, u32[]{:S(2)}, u32[]{:S(2)}) %all-to-all-start) | async-done | bytes 131104 | tf_op jit(solution)/shard_map/all_to_all | solution.py:289
  64.7 0.0 copy-done.9
  64.7 0.3 fusion.5
  65.0 0.0 copy-done
  65.0 0.0 copy-done.10
  65.0 1.2 %convolution_convert_fusion = bf16[64,1024]{1,0:T(8,128)(2,1)} fusion(bf16[1,512,1024]{2,1,0:T(8,128)(2,1)S(1)} %copy-done, bf16[1,1024,512]{2,1,0:T(8,128)(2,1)S(1)} %copy-done.10, bf16[8,8,1024]{2,1,0:T(8,128)(2,1)S(1)} %all-to-all-done, f32[64,512]{1,0:T(8,128)S(1)} %fusion.5), kind=kOutput, calls=%fused_computation.1 | convolution fusion | flops 134479872 | bytes 2490368 | tf_op jit(solution)/shard_map/dot_general | solution.py:229
  66.2 0.0 reduce-scatter.2.cloned.1.call-update
  66.2 0.1 copy.30
  66.3 0.1 mul.76
  66.4 0.1 copy.29
  66.5 0.0 copy-done.12
  66.5 0.1 copy.26
  66.6 21.3 %reduce-scatter.2.cloned.1.call-done = bf16[64,256]{1,0:T(8,128)(2,1)} async-done(((bf16[64,1024]{1,0:T(8,128)(2,1)}), bf16[64,256]{1,0:T(8,128)(2,1)}) %reduce-scatter.2.cloned.1.call-update) | async-done | bytes 32784 | tf_op jit(solution)/shard_map/reduce_scatter | solution.py:230
  87.8 4.6 %all-to-all-start.1 = ((bf16[8,8,256]{2,1,0:T(8,128)(2,1)}), bf16[8,8,256]{2,1,0:T(8,128)(2,1)S(1)}, u32[]{:S(2)}, u32[]{:S(2)}) async-start(bf16[8,8,256]{2,1,0:T(8,128)(2,1)} %bitcast.31), calls=%async_computation.2 | async-start | bytes 65536 | tf_op jit(solution)/shard_map/all_to_all | solution.py:295
  92.4 5.7 %all-to-all-done.1 = bf16[8,8,256]{2,1,0:T(8,128)(2,1)S(1)} async-done(((bf16[8,8,256]{2,1,0:T(8,128)(2,1)}), bf16[8,8,256]{2,1,0:T(8,128)(2,1)S(1)}, u32[]{:S(2)}, u32[]{:S(2)}) %all-to-all-start.1) | async-done | bytes 32800 | tf_op jit(solution)/shard_map/all_to_all | solution.py:295
  98.2 0.6 gather_fusion
  98.8 0.1 multiply_reduce_fusion.1
  98.9 0.6 add_convert_fusion
  (7 shorter events, 0.1 us)
Async XLA Ops:
  7.2 57.8 %copy-start = (bf16[1,512,1024]{2,1,0:T(8,128)(2,1)S(1)}, bf16[1,512,1024]{2,1,0:T(8,128)(2,1)}, u32[]{:S(2)}) copy-start(bf16[1,512,1024]{2,1,0:T(8,128)(2,1)} %param.29) | copy-start | bytes 3145732
  7.2 50.9 %copy-start.11 = (s32[16,2]{0,1:T(2,128)S(1)}, s32[16,2]{0,1:T(2,128)}, u32[]{:S(2)}) copy-start(s32[16,2]{0,1:T(2,128)} %param.25) | copy-start | bytes 388
  7.2 43.3 %copy-start.6 = (bf16[16,1024]{1,0:T(8,128)(2,1)S(1)}, bf16[16,1024]{1,0:T(8,128)(2,1)}, u32[]{:S(2)}) copy-start(bf16[16,1024]{1,0:T(8,128)(2,1)} %tokens_ref.1) | copy-start | bytes 98308
  7.2 43.4 %copy-start.13 = (f32[1024]{0:T(1024)S(1)}, f32[1024]{0:T(1024)}, u32[]{:S(2)}) copy-start(f32[1024]{0:T(1024)} %param.24) | copy-start | bytes 12292
  7.2 59.3 %copy-start.12 = (f32[16,2]{0,1:T(2,128)S(1)}, f32[16,2]{0,1:T(2,128)}, u32[]{:S(2)}) copy-start(f32[16,2]{0,1:T(2,128)} %param.26) | copy-start | bytes 388
  9.8 1.0 copy-start.1
  10.9 1.0 copy-start.2
  11.9 1.0 copy-start.3
  13.0 1.0 copy-start.4
  14.0 0.8 copy-start.5
  14.8 0.7 copy-start.7
  15.5 0.7 copy-start.8
  16.1 48.5 %copy-start.9 = (bf16[1,1024,512]{2,1,0:T(8,128)(2,1)S(1)}, bf16[1,1024,512]{2,1,0:T(8,128)(2,1)}, u32[]{:S(2)}) copy-start(bf16[1,1024,512]{2,1,0:T(8,128)(2,1)} %param.27) | copy-start | bytes 3145732
  16.1 48.9 %copy-start.10 = (bf16[1,1024,512]{2,1,0:T(8,128)(2,1)S(1)}, bf16[1,1024,512]{2,1,0:T(8,128)(2,1)}, u32[]{:S(2)}) copy-start(bf16[1,1024,512]{2,1,0:T(8,128)(2,1)} %param.28) | copy-start | bytes 3145732
  51.7 12.9 %all-to-all-start = ((bf16[8,8,1024]{2,1,0:T(8,128)(2,1)}), bf16[8,8,1024]{2,1,0:T(8,128)(2,1)S(1)}, u32[]{:S(2)}, u32[]{:S(2)}) async-start(bf16[8,8,1024]{2,1,0:T(8,128)(2,1)} %fusion), calls=%async_computation | async-start | bytes 262144 | tf_op jit(solution)/shard_map/all_to_all | solution.py:289
  57.9 29.9 %reduce-scatter.2.cloned.1.call-start = ((), (), s32[]{:S(2)}) async-start(), calls=%async_computation.3 | async-start | bytes 163840 | tf_op jit(solution)/shard_map/reduce_scatter | solution.py:230
  87.8 10.3 %all-to-all-start.1 = ((bf16[8,8,256]{2,1,0:T(8,128)(2,1)}), bf16[8,8,256]{2,1,0:T(8,128)(2,1)S(1)}, u32[]{:S(2)}, u32[]{:S(2)}) async-start(bf16[8,8,256]{2,1,0:T(8,128)(2,1)} %bitcast.31), calls=%async_computation.2 | async-start | bytes 65536 | tf_op jit(solution)/shard_map/all_to_all | solution.py:295
Sparse Core Ops, SparseCore 0:
  66.3 21.4 reduce-scatter.1
